TPU v7x, 32 devices: a whole 2x2x4 slice. The times are simulated.
32 devices in a mesh: ep: 4 (over y, x), tp: 8 (over z, core).
Axes of the slice: x: 2, y: 2, z: 4, core: 2. Of those that a mesh axis runs over, the one named last changes fastest.
Arguments:
- tokens: bfloat16 [1024, 2048], P('ep', 'tp'), may hold values from -600 to 600
- pre_gain: float32 [2048], P('tp'), may hold values from 0.1 to 1.9
- expert_gate: bfloat16 [4, 2048, 8192], P('ep', None, 'tp'), may hold values from -0.125 to 0.125
- expert_up: bfloat16 [4, 2048, 8192], P('ep', None, 'tp'), may hold values from -0.125 to 0.125
- expert_down: bfloat16 [4, 8192, 2048], P('ep', 'tp'), may hold values from -8 to 8
- routes: int32 [1024, 2], P('ep'), may hold values from 0 to 3, all different within a row; in each aligned block of 256 rows (0 to 255, 256 to 511, ...) at most 192 rows name the same one
- route_weights: float32 [1024, 2], P('ep'), may hold values from 0.1 to 1
- post_gain: float32 [2048], P('tp'), may hold values from 0.1 to 1.9
Outputs:
- layer_out: bfloat16 [1024, 2048], P('ep', 'tp')
Inputs may be any that keep to these rules, and one draw needn't show every extreme that they name: `routes`: each token names 2 different experts. Among the 256 tokens of one index of ep no expert is named more than 192 times, a bound that some expert reaches in some of these blocks.
All inputs are finite; a program needn't handle non-finite values.
Results may differ from a plain program's by a relative error of at most 0.024.
Values may be sent and summed in bfloat16 or wider, within the bound.
A program may use at most 64 MiB of HBM per device.

v0:
```python
import jax
import jax.numpy as jnp
from jax import lax
from jax.sharding import PartitionSpec as P

EPSILON = 1e-06


def local(tokens, pre_gain, expert_gate, expert_up, expert_down, routes, route_weights, post_gain):
    local_experts = expert_gate.shape[0]
    groups = lax.axis_size("ep")
    experts_all = local_experts * groups
    tok_rows, part_width = tokens.shape
    full_width = part_width * lax.axis_size("tp")
    capacity = 3 * tok_rows // experts_all
    values = tokens.astype(jnp.float32)
    input_sq = lax.psum(jnp.sum(values * values, axis=-1), "tp")
    normed = (
        values * lax.rsqrt(input_sq / full_width + EPSILON)[:, None] * pre_gain[None, :]
    ).astype(jnp.bfloat16)
    onehot = (routes[:, :, None] == jnp.arange(experts_all, dtype=jnp.int32)).astype(jnp.int32)
    onehot = onehot.reshape(tok_rows * 2, experts_all)
    earlier = jnp.cumsum(onehot, axis=0) - onehot
    slots = jnp.sum(earlier * onehot, axis=-1).reshape(tok_rows, 2)
    positions = routes * capacity + slots
    places = jnp.arange(experts_all * capacity, dtype=jnp.int32)
    first_pick = (places[:, None] == positions[None, :, 0]).astype(jnp.bfloat16)
    second_pick = (places[:, None] == positions[None, :, 1]).astype(jnp.bfloat16)
    dispatch = first_pick + second_pick
    outgoing = jnp.dot(dispatch, normed, preferred_element_type=jnp.float32).astype(jnp.bfloat16)
    arrived = lax.all_to_all(outgoing, "ep", split_axis=0, concat_axis=0, tiled=True)
    fragment = lax.all_gather(arrived, "tp", axis=1, tiled=True)
    count = fragment.shape[1]
    grouped = fragment.reshape(groups, local_experts, capacity, count)
    gate_pre = jnp.einsum(
        "secw,ewf->secf", grouped, expert_gate, preferred_element_type=jnp.float32
    )
    up_pre = jnp.einsum("secw,ewf->secf", grouped, expert_up, preferred_element_type=jnp.float32)
    hidden = (jax.nn.silu(gate_pre) * up_pre).astype(jnp.bfloat16)
    product = jnp.einsum("secf,efd->dsec", hidden, expert_down, preferred_element_type=jnp.float32)
    summed = lax.psum_scatter(
        product.reshape(lax.axis_size("tp") * part_width, groups * local_experts * capacity).astype(
            jnp.bfloat16
        ),
        "tp",
        scatter_dimension=0,
        tiled=True,
    )
    returned = lax.all_to_all(summed, "ep", split_axis=1, concat_axis=1, tiled=True)
    contract = (((0,), (1,)), ((), ()))
    first_out = lax.dot_general(first_pick, returned, contract, preferred_element_type=jnp.float32)
    second_out = lax.dot_general(
        second_pick, returned, contract, preferred_element_type=jnp.float32
    )
    combined = route_weights[:, 0:1] * first_out + route_weights[:, 1:2] * second_out
    output_sq = lax.psum(jnp.sum(combined * combined, axis=-1), "tp")
    scaled = combined * lax.rsqrt(output_sq / full_width + EPSILON)[:, None] * post_gain[None, :]
    return scaled.astype(jnp.bfloat16)


def solution(mesh):
    placed = (
        P("ep", "tp"),
        P("tp"),
        P("ep", None, "tp"),
        P("ep", None, "tp"),
        P("ep", "tp", None),
        P("ep", None),
        P("ep", None),
        P("tp"),
    )
    return jax.shard_map(
        local, mesh=mesh, in_specs=placed, out_specs=P("ep", "tp"), check_vma=False
    )
```

profile of v0, /device:TPU:0, one launch (start us, length us, event | category | flops | bytes accessed | tf_op | source)
XLA Modules:
  0.0 164.0 jit_solution(8557718616161930768)
XLA Ops:
  6.5 0.0 all-gather.2.cloned.1.call-start
  6.5 0.8 copy.20
  7.4 0.1 eq.61
  7.5 0.1 eq.57
  7.7 1.2 reduce-window.6
  8.9 0.2 slice_reduce_fusion
  9.1 0.2 reduce-window.9
  9.3 0.1 add_bitcast_fusion
  9.4 0.1 reshape.55
  9.5 0.1 copy.22
  9.6 0.7 multiply_add_fusion
  10.3 1.0 fusion.28
  11.3 18.1 %psum.14 = f32[256]{0:T(256)S(1)} all-reduce(f32[256]{0:T(256)S(1)} %fusion.28), channel_id=1, replica_groups=mesh['ep'=4,'tp'=8] {'tp'}, use_global_device_ids=true, to_apply=%region_4.5 | all-reduce | flops 256 | bytes 2048 | tf_op jit(solution)/shard_map/psum | solution.py:17
  29.4 1.3 convolution_convert_fusion
  30.7 10.1 %all_to_all.24 = bf16[4,192,256]{2,1,0:T(8,128)(2,1)} all-to-all(bf16[4,192,256]{2,1,0:T(8,128)(2,1)S(1)} %bitcast.82), channel_id=1, replica_groups=mesh['ep'=4,'tp'=8] {'ep'}, dimensions={0} | all-to-all | bytes 786432 | tf_op jit(solution)/shard_map/all_to_all | solution.py:31
  40.8 0.0 all-gather.2.cloned.1.call-update
  40.8 0.0 reduce-scatter.2.cloned.1.call-start
  40.8 35.9 %all-gather.2.cloned.1.call-done = bf16[768,2048]{1,0:T(8,128)(2,1)} async-done(((bf16[768,256]{1,0:T(8,128)(2,1)}), bf16[768,2048]{1,0:T(8,128)(2,1)}) %all-gather.2.cloned.1.call-update) | async-done | bytes 3145744 | tf_op jit(solution)/shard_map/all_gather | solution.py:32
  76.8 0.0 copy-start.2
  76.8 0.0 copy-start.4
  76.8 6.3 %fusion.2 = f32[4,192,1024]{2,1,0:T(8,128)S(1)} fusion(bf16[4,192,2048]{2,1,0:T(8,128)(2,1)} %bitcast.90, bf16[1,2048,1024]{2,1,0:T(8,128)(2,1)} %param.11), kind=kOutput, calls=%fused_computation.2 | convolution fusion | flops 3221225472 | bytes 10485760 | tf_op jit(solution)/shard_map/secw,ewf->secf/dot_general | solution.py:38
  83.1 0.0 copy-done.2
  83.1 0.0 copy-done.4
  83.1 0.0 copy-start.3
  83.1 3.8 %fusion.9 = bf16[4,1,192,1024]{3,2,0,1:T(8,128)(2,1)S(1)} fusion(f32[4,192,1024]{2,1,0:T(8,128)S(1)} %fusion.2, bf16[4,192,2048]{2,1,0:T(8,128)(2,1)S(1)} %bitcast.91, bf16[1,2048,1024]{2,1,0:T(8,128)(2,1)S(1)} %copy-done.2), kind=kOutput, calls=%fused_computation.8 | convolution fusion | flops 3225944064 | bytes 12058624 | tf_op jit(solution)/shard_map/secw,ewf->secf/dot_general | solution.py:35
  87.0 0.0 copy-done.3
  87.0 4.8 %fusion.13 = bf16[2048,768]{0,1:T(8,128)(2,1)} fusion(bf16[768,1024]{1,0:T(8,128)(2,1)S(1)} %bitcast.92, bf16[1,1024,2048]{2,1,0:T(8,128)(2,1)S(1)} %copy-done.3), kind=kOutput, calls=%fused_computation.14 | convolution fusion | flops 3222798336 | bytes 8912896 | tf_op jit(solution)/shard_map/secf,efd->dsec/dot_general | solution.py:40
  91.8 0.0 copy-start
  91.8 0.0 copy-start.1
  91.8 0.0 reduce-scatter.2.cloned.1.call-update
  91.8 38.8 %reduce-scatter.2.cloned.1.call-done = bf16[256,768]{0,1:T(8,128)(2,1)} async-done(((bf16[2048,768]{0,1:T(8,128)(2,1)}), bf16[256,768]{0,1:T(8,128)(2,1)}) %reduce-scatter.2.cloned.1.call-update) | async-done | bytes 393232 | tf_op jit(solution)/shard_map/reduce_scatter | solution.py:41
  130.6 3.6 %all-to-all-start.1 = ((bf16[256,4,192]{0,2,1:T(8,128)(2,1)}), bf16[256,4,192]{0,2,1:T(8,128)(2,1)S(1)}, u32[]{:S(2)}, u32[]{:S(2)}) async-start(bf16[256,4,192]{0,2,1:T(8,128)(2,1)} %bitcast.81), calls=%async_computation.2 | async-start | bytes 786432 | tf_op jit(solution)/shard_map/all_to_all | solution.py:49
  134.2 0.0 copy-done
  134.2 5.9 %all-to-all-done.1 = bf16[256,4,192]{0,2,1:T(8,128)(2,1)S(1)} async-done(((bf16[256,4,192]{0,2,1:T(8,128)(2,1)}), bf16[256,4,192]{0,2,1:T(8,128)(2,1)S(1)}, u32[]{:S(2)}, u32[]{:S(2)}) %all-to-all-start.1) | async-done | bytes 393248 | tf_op jit(solution)/shard_map/all_to_all | solution.py:49
  140.1 0.4 convolution_multiply_fusion.1
  140.5 0.4 multiply_reduce_fusion
  140.9 15.4 %psum.15 = f32[256]{0:T(256)S(1)} all-reduce(f32[256]{0:T(256)S(1)} %get-tuple-element.9), channel_id=1, replica_groups=mesh['ep'=4,'tp'=8] {'tp'}, use_global_device_ids=true, to_apply=%region_7.8 | all-reduce | flops 256 | bytes 2048 | tf_op jit(solution)/shard_map/psum | solution.py:56
  156.3 0.0 copy-done.1
  156.3 0.1 multiply_convert_fusion
  156.4 0.8 copy.23
  (6 shorter events, 0.1 us)
Async XLA Ops:
  6.5 70.3 %all-gather.2.cloned.1.call-start = ((), (), s32[]{:S(2)}) async-start(), calls=%async_computation.3 | async-start | bytes 3538944 | tf_op jit(solution)/shard_map/all_gather | solution.py:32
  40.8 89.8 %reduce-scatter.2.cloned.1.call-start = ((), (), s32[]{:S(2)}) async-start(), calls=%async_computation.4 | async-start | bytes 3538944 | tf_op jit(solution)/shard_map/reduce_scatter | solution.py:41
  76.8 6.3 %copy-start.2 = (bf16[1,2048,1024]{2,1,0:T(8,128)(2,1)S(1)}, bf16[1,2048,1024]{2,1,0:T(8,128)(2,1)}, u32[]{:S(2)}) copy-start(bf16[1,2048,1024]{2,1,0:T(8,128)(2,1)} %param.10) | copy-start | bytes 12582916
  76.8 6.3 %copy-start.4 = (bf16[768,2048]{1,0:T(8,128)(2,1)S(1)}, bf16[768,2048]{1,0:T(8,128)(2,1)}, u32[]{:S(2)}) copy-start(bf16[768,2048]{1,0:T(8,128)(2,1)} %all-gather.2.cloned.1.call-done) | copy-start | bytes 9437188
  83.1 3.9 %copy-start.3 = (bf16[1,1024,2048]{2,1,0:T(8,128)(2,1)S(1)}, bf16[1,1024,2048]{2,1,0:T(8,128)(2,1)}, u32[]{:S(2)}) copy-start(bf16[1,1024,2048]{2,1,0:T(8,128)(2,1)} %param.12) | copy-start | bytes 12582916
  91.8 42.4 %copy-start = (f32[256,2]{0,1:T(2,128)S(1)}, f32[256,2]{0,1:T(2,128)}, u32[]{:S(2)}) copy-start(f32[256,2]{0,1:T(2,128)} %param.14) | copy-start | bytes 6148
  91.8 64.5 %copy-start.1 = (f32[256]{0:T(256)S(1)}, f32[256]{0:T(256)}, u32[]{:S(2)}) copy-start(f32[256]{0:T(256)} %param.15) | copy-start | bytes 3076
  130.6 9.5 %all-to-all-start.1 = ((bf16[256,4,192]{0,2,1:T(8,128)(2,1)}), bf16[256,4,192]{0,2,1:T(8,128)(2,1)S(1)}, u32[]{:S(2)}, u32[]{:S(2)}) async-start(bf16[256,4,192]{0,2,1:T(8,128)(2,1)} %bitcast.81), calls=%async_computation.2 | async-start | bytes 786432 | tf_op jit(solution)/shard_map/all_to_all | solution.py:49
Sparse Core Ops, SparseCore 0:
  40.9 35.8 all-gather.1
  91.9 38.5 reduce-scatter.1
where the time goes:
time: 164 us
  waiting for transfers between devices  80.6 us (49%)
  blocking collectives  43.6 us (27%)
  matrix products  17 us (10%)
  between operations  13.5 us (8%)
  starting transfers between devices  3.69 us (2%)
  other arithmetic  3.35 us (2%)
  local copies, waits for them, and re-layouts  2.31 us (1%)
    reduce_scatter x1, waiting for transfers between devices, local(): lax.psum_scatter(product.reshape(lax.axis_size('tp') * part_width, groups...  38.8 us
    all_gather x1, waiting for transfers between devices, local(): fragment = lax.all_gather(arrived, 'tp', axis=1, tiled=True)  35.9 us
    psum x1, blocking collectives, local(): input_sq = lax.psum(jnp.sum(values * values, axis=-1), 'tp')  18.1 us
    psum x1, blocking collectives, local(): output_sq = lax.psum(jnp.sum(combined * combined, axis=-1), 'tp')  15.4 us
    all_to_all x1, blocking collectives, local(): lax.all_to_all(outgoing, 'ep', split_axis=0, concat_axis=0, tiled=True)  10.1 us
    dot_general x1, matrix products, local(): jnp.einsum('secw,ewf->secf', grouped, expert_up, preferred_element_type=j...  6.28 us
    all_to_all x1, waiting for transfers between devices, local(): lax.all_to_all(summed, 'ep', split_axis=1, concat_axis=1, tiled=True)  5.87 us
    dot_general x1, matrix products, local(): jnp.einsum('secf,efd->dsec', hidden, expert_down, preferred_element_type=...  4.83 us
  transfers between devices with their start and end apart: 3, of which 3 were waited for; matrix products, arithmetic and copies ran while one was open for 0% of the time, Pallas kernels for 0%

commit v1 on v0

--- a/solution.py
+++ b/solution.py
@@ -29,7 +29,12 @@
     dispatch = first_pick + second_pick
     outgoing = jnp.dot(dispatch, normed, preferred_element_type=jnp.float32).astype(jnp.bfloat16)
     arrived = lax.all_to_all(outgoing, "ep", split_axis=0, concat_axis=0, tiled=True)
-    fragment = lax.all_gather(arrived, "tp", axis=1, tiled=True)
+    ring = [arrived]
+    for hop in range(7):
+        ring.append(lax.ppermute(ring[-1], "tp", [(dev, (dev + 1) % 8) for dev in range(8)]))
+    fragment = jnp.roll(
+        jnp.concatenate(ring[::-1], axis=1), (lax.axis_index("tp") + 1) * ring[0].shape[1], axis=1
+    )
     count = fragment.shape[1]
     grouped = fragment.reshape(groups, local_experts, capacity, count)
     gate_pre = jnp.einsum(

time: 164 us -> 189 us (1.15)
  waiting for transfers between devices: 80.6 us -> 106 us
  matrix products: 17 us -> 13.9 us
  local copies, waits for them, and re-layouts: 2.31 us -> 4.81 us
    ppermute x0 -> x7, waiting for transfers between devices: none -> 63 us  [local(): lax.ppermute(ring[-1], 'tp', [(dev, (dev + 1) % 8) for dev in range(8)])]
    all_gather x1 -> x0, waiting for transfers between devices: 35.9 us -> none  [local(): fragment = lax.all_gather(arrived, 'tp', axis=1, tiled=True)]
    dot_general x1, matrix products: 6.28 us -> 3.6 us  [local(): jnp.einsum('secw,ewf->secf', grouped, expert_up, preferred_element_type=j...]
    unnamed x11 -> x26, local copies, waits for them, and re-layouts: 0.83 us -> 2.88 us
  transfers between devices with their start and end apart: 3 -> 9, of which waited for: 3 -> 9; matrix products, arithmetic and copies ran while one was open for 0% -> 0% of each run, Pallas kernels for 0% -> 0%
where the time goes in v1:
time: 189 us
  waiting for transfers between devices  106 us (56%)
  blocking collectives  43.5 us (23%)
  matrix products  13.9 us (7%)
  between operations  13.7 us (7%)
  local copies, waits for them, and re-layouts  4.81 us (3%)
  starting transfers between devices  3.67 us (2%)
  other arithmetic  3.35 us (2%)
    ppermute x7, waiting for transfers between devices, local(): lax.ppermute(ring[-1], 'tp', [(dev, (dev + 1) % 8) for dev in range(8)])  63 us
    reduce_scatter x1, waiting for transfers between devices, local(): lax.psum_scatter(product.reshape(lax.axis_size('tp') * part_width, groups...  37.2 us
    psum x1, blocking collectives, local(): input_sq = lax.psum(jnp.sum(values * values, axis=-1), 'tp')  18.1 us
    psum x1, blocking collectives, local(): output_sq = lax.psum(jnp.sum(combined * combined, axis=-1), 'tp')  15.4 us
    all_to_all x1, blocking collectives, local(): lax.all_to_all(outgoing, 'ep', split_axis=0, concat_axis=0, tiled=True)  9.95 us
    all_to_all x1, waiting for transfers between devices, local(): lax.all_to_all(summed, 'ep', split_axis=1, concat_axis=1, tiled=True)  5.87 us
    dot_general x1, matrix products, local(): jnp.einsum('secf,efd->dsec', hidden, expert_down, preferred_element_type=...  4.85 us
  transfers between devices with their start and end apart: 9, of which 9 were waited for; matrix products, arithmetic and copies ran while one was open for 0% of the time, Pallas kernels for 0%

profile of v1, /device:TPU:0, one launch (start us, length us, event | category | flops | bytes accessed | tf_op | source)
XLA Modules:
  0.0 188.9 jit_solution(16544853255921995644)
XLA Ops:
  6.5 0.0 reduce-scatter.2.cloned.1.call-start
  6.5 0.8 copy.20
  7.4 0.1 eq.64
  7.5 0.1 eq.60
  7.7 1.2 reduce-window.6
  8.9 0.2 slice_reduce_fusion
  9.1 0.2 reduce-window.9
  9.3 0.1 add_bitcast_fusion
  9.4 0.1 reshape.55
  9.5 0.1 copy.22
  9.6 0.7 multiply_add_fusion
  10.3 1.0 fusion.28
  11.3 18.1 %psum.14 = f32[256]{0:T(256)S(1)} all-reduce(f32[256]{0:T(256)S(1)} %fusion.28), channel_id=1, replica_groups=mesh['ep'=4,'tp'=8] {'tp'}, use_global_device_ids=true, to_apply=%region_4.5 | all-reduce | flops 256 | bytes 2048 | tf_op jit(solution)/shard_map/psum | solution.py:17
  29.4 1.3 convolution_convert_fusion
  30.7 9.9 %all_to_all.24 = bf16[4,192,256]{2,1,0:T(8,128)(2,1)S(1)} all-to-all(bf16[4,192,256]{2,1,0:T(8,128)(2,1)S(1)} %bitcast.86), channel_id=1, replica_groups=mesh['ep'=4,'tp'=8] {'ep'}, dimensions={0} | all-to-all | bytes 786432 | tf_op jit(solution)/shard_map/all_to_all | solution.py:31
  40.7 0.0 collective-permute-start
  40.7 9.0 %collective-permute-done = bf16[768,256]{1,0:T(8,128)(2,1)S(1)} collective-permute-done((bf16[768,256]{1,0:T(8,128)(2,1)S(1)}, bf16[768,256]{1,0:T(8,128)(2,1)S(1)}, u32[]{:S(2)}, u32[]{:S(2)}) %collective-permute-start) | collective-permute-done | bytes 393248 | tf_op jit(solution)/shard_map/ppermute | solution.py:34
  49.7 0.0 collective-permute-start.1
  49.7 9.0 %collective-permute-done.1 = bf16[768,256]{1,0:T(8,128)(2,1)S(1)} collective-permute-done((bf16[768,256]{1,0:T(8,128)(2,1)S(1)}, bf16[768,256]{1,0:T(8,128)(2,1)S(1)}, u32[]{:S(2)}, u32[]{:S(2)}) %collective-permute-start.1) | collective-permute-done | bytes 393248 | tf_op jit(solution)/shard_map/ppermute | solution.py:34
  58.7 0.0 collective-permute-start.2
  58.7 9.0 %collective-permute-done.2 = bf16[768,256]{1,0:T(8,128)(2,1)S(1)} collective-permute-done((bf16[768,256]{1,0:T(8,128)(2,1)S(1)}, bf16[768,256]{1,0:T(8,128)(2,1)S(1)}, u32[]{:S(2)}, u32[]{:S(2)}) %collective-permute-start.2) | collective-permute-done | bytes 393248 | tf_op jit(solution)/shard_map/ppermute | solution.py:34
  67.7 0.0 collective-permute-start.3
  67.7 9.0 %collective-permute-done.3 = bf16[768,256]{1,0:T(8,128)(2,1)S(1)} collective-permute-done((bf16[768,256]{1,0:T(8,128)(2,1)S(1)}, bf16[768,256]{1,0:T(8,128)(2,1)S(1)}, u32[]{:S(2)}, u32[]{:S(2)}) %collective-permute-start.3) | collective-permute-done | bytes 393248 | tf_op jit(solution)/shard_map/ppermute | solution.py:34
  76.7 0.0 collective-permute-start.4
  76.7 9.0 %collective-permute-done.4 = bf16[768,256]{1,0:T(8,128)(2,1)S(1)} collective-permute-done((bf16[768,256]{1,0:T(8,128)(2,1)S(1)}, bf16[768,256]{1,0:T(8,128)(2,1)S(1)}, u32[]{:S(2)}, u32[]{:S(2)}) %collective-permute-start.4) | collective-permute-done | bytes 393248 | tf_op jit(solution)/shard_map/ppermute | solution.py:34
  85.7 0.0 collective-permute-start.5
  85.7 9.0 %collective-permute-done.5 = bf16[768,256]{1,0:T(8,128)(2,1)S(1)} collective-permute-done((bf16[768,256]{1,0:T(8,128)(2,1)S(1)}, bf16[768,256]{1,0:T(8,128)(2,1)S(1)}, u32[]{:S(2)}, u32[]{:S(2)}) %collective-permute-start.5) | collective-permute-done | bytes 393248 | tf_op jit(solution)/shard_map/ppermute | solution.py:34
  94.7 0.0 collective-permute-start.6
  94.7 9.0 %collective-permute-done.6 = bf16[768,256]{1,0:T(8,128)(2,1)S(1)} collective-permute-done((bf16[768,256]{1,0:T(8,128)(2,1)S(1)}, bf16[768,256]{1,0:T(8,128)(2,1)S(1)}, u32[]{:S(2)}, u32[]{:S(2)}) %collective-permute-start.6) | collective-permute-done | bytes 393248 | tf_op jit(solution)/shard_map/ppermute | solution.py:34
  104.1 0.0 copy-start.2
  104.6 0.4 constant_dynamic-slice_fusion
  105.0 1.3 copy-done.2
  106.3 3.4 %fusion.4 = f32[4,192,1024]{2,1,0:T(8,128)S(1)} fusion(bf16[4,192,2048]{2,1,0:T(8,128)(2,1)S(1)} %bitcast.81, bf16[1,2048,1024]{2,1,0:T(8,128)(2,1)S(1)} %copy-done.2), kind=kOutput, calls=%fused_computation.4 | convolution fusion | flops 3221225472 | bytes 10485760 | tf_op jit(solution)/shard_map/secw,ewf->secf/dot_general | solution.py:40
  109.7 0.0 copy-start.4
  109.7 3.6 %fusion.9 = bf16[4,1,192,1024]{3,2,0,1:T(8,128)(2,1)S(1)} fusion(f32[4,192,1024]{2,1,0:T(8,128)S(1)} %fusion.4, bf16[4,192,2048]{2,1,0:T(8,128)(2,1)S(1)} %bitcast.82, bf16[1,2048,1024]{2,1,0:T(8,128)(2,1)S(1)} %copy-done.3), kind=kOutput, calls=%fused_computation.8 | convolution fusion | flops 3225944064 | bytes 12058624 | tf_op jit(solution)/shard_map/secw,ewf->secf/dot_general | solution.py:43
  113.4 0.0 copy-start
  113.4 0.0 copy-start.1
  113.4 4.8 %fusion.13 = bf16[2048,768]{0,1:T(8,128)(2,1)} fusion(bf16[768,1024]{1,0:T(8,128)(2,1)S(1)} %bitcast.94, bf16[1,1024,2048]{2,1,0:T(8,128)(2,1)S(1)} %copy-done.4), kind=kOutput, calls=%fused_computation.14 | convolution fusion | flops 3222798336 | bytes 8912896 | tf_op jit(solution)/shard_map/secf,efd->dsec/dot_general | solution.py:45
  118.2 0.0 reduce-scatter.2.cloned.1.call-update
  118.3 37.2 %reduce-scatter.2.cloned.1.call-done = bf16[256,768]{0,1:T(8,128)(2,1)} async-done(((bf16[2048,768]{0,1:T(8,128)(2,1)}), bf16[256,768]{0,1:T(8,128)(2,1)}) %reduce-scatter.2.cloned.1.call-update) | async-done | bytes 393232 | tf_op jit(solution)/shard_map/reduce_scatter | solution.py:46
  155.4 3.6 %all-to-all-start.1 = ((bf16[256,4,192]{0,2,1:T(8,128)(2,1)}), bf16[256,4,192]{0,2,1:T(8,128)(2,1)S(1)}, u32[]{:S(2)}, u32[]{:S(2)}) async-start(bf16[256,4,192]{0,2,1:T(8,128)(2,1)} %bitcast.85), calls=%async_computation.2 | async-start | bytes 786432 | tf_op jit(solution)/shard_map/all_to_all | solution.py:54
  159.1 0.0 copy-done
  159.1 5.9 %all-to-all-done.1 = bf16[256,4,192]{0,2,1:T(8,128)(2,1)S(1)} async-done(((bf16[256,4,192]{0,2,1:T(8,128)(2,1)}), bf16[256,4,192]{0,2,1:T(8,128)(2,1)S(1)}, u32[]{:S(2)}, u32[]{:S(2)}) %all-to-all-start.1) | async-done | bytes 393248 | tf_op jit(solution)/shard_map/all_to_all | solution.py:54
  165.0 0.4 convolution_multiply_fusion.1
  165.3 0.4 multiply_reduce_fusion
  165.7 15.4 %psum.15 = f32[256]{0:T(256)S(1)} all-reduce(f32[256]{0:T(256)S(1)} %get-tuple-element.9), channel_id=1, replica_groups=mesh['ep'=4,'tp'=8] {'tp'}, use_global_device_ids=true, to_apply=%region_7.8 | all-reduce | flops 256 | bytes 2048 | tf_op jit(solution)/shard_map/psum | solution.py:61
  181.1 0.1 multiply_convert_fusion
  181.3 0.8 copy.23
  (26 shorter events, 0.8 us)
Async XLA Ops:
  6.5 148.9 %reduce-scatter.2.cloned.1.call-start = ((), (), s32[]{:S(2)}) async-start(), calls=%async_computation.3 | async-start | bytes 3538944 | tf_op jit(solution)/shard_map/reduce_scatter | solution.py:46
  40.7 9.0 %collective-permute-start = (bf16[768,256]{1,0:T(8,128)(2,1)S(1)}, bf16[768,256]{1,0:T(8,128)(2,1)S(1)}, u32[]{:S(2)}, u32[]{:S(2)}) collective-permute-start(bf16[768,256]{1,0:T(8,128)(2,1)S(1)} %bitcast.78), channel_id=1, source_target_pairs={{0,1},{1,2},{2,3},{3,4},{4,5},{5,6},{6,7},{7,0},{8,9},{9,10},{10,1... | collective-permute-start | bytes 1179656 | tf_op jit(solution)/shard_map/ppermute | solution.py:34
  49.7 9.0 %collective-permute-start.1 = (bf16[768,256]{1,0:T(8,128)(2,1)S(1)}, bf16[768,256]{1,0:T(8,128)(2,1)S(1)}, u32[]{:S(2)}, u32[]{:S(2)}) collective-permute-start(bf16[768,256]{1,0:T(8,128)(2,1)S(1)} %collective-permute-done), channel_id=1, source_target_pairs={{0,1},{1,2},{2,3},{3,4},{4,5},{5,6},{6,7},{7,0},{8,9},{9,10},{10,1... | collective-permute-start | bytes 1179656 | tf_op jit(solution)/shard_map/ppermute | solution.py:34
  58.7 9.0 %collective-permute-start.2 = (bf16[768,256]{1,0:T(8,128)(2,1)S(1)}, bf16[768,256]{1,0:T(8,128)(2,1)S(1)}, u32[]{:S(2)}, u32[]{:S(2)}) collective-permute-start(bf16[768,256]{1,0:T(8,128)(2,1)S(1)} %collective-permute-done.1), channel_id=1, source_target_pairs={{0,1},{1,2},{2,3},{3,4},{4,5},{5,6},{6,7},{7,0},{8,9},{9,10},{10,1... | collective-permute-start | bytes 1179656 | tf_op jit(solution)/shard_map/ppermute | solution.py:34
  67.7 9.0 %collective-permute-start.3 = (bf16[768,256]{1,0:T(8,128)(2,1)S(1)}, bf16[768,256]{1,0:T(8,128)(2,1)S(1)}, u32[]{:S(2)}, u32[]{:S(2)}) collective-permute-start(bf16[768,256]{1,0:T(8,128)(2,1)S(1)} %collective-permute-done.2), channel_id=1, source_target_pairs={{0,1},{1,2},{2,3},{3,4},{4,5},{5,6},{6,7},{7,0},{8,9},{9,10},{10,1... | collective-permute-start | bytes 1179656 | tf_op jit(solution)/shard_map/ppermute | solution.py:34
  76.7 9.0 %collective-permute-start.4 = (bf16[768,256]{1,0:T(8,128)(2,1)S(1)}, bf16[768,256]{1,0:T(8,128)(2,1)S(1)}, u32[]{:S(2)}, u32[]{:S(2)}) collective-permute-start(bf16[768,256]{1,0:T(8,128)(2,1)S(1)} %collective-permute-done.3), channel_id=1, source_target_pairs={{0,1},{1,2},{2,3},{3,4},{4,5},{5,6},{6,7},{7,0},{8,9},{9,10},{10,1... | collective-permute-start | bytes 1179656 | tf_op jit(solution)/shard_map/ppermute | solution.py:34
  85.7 9.0 %collective-permute-start.5 = (bf16[768,256]{1,0:T(8,128)(2,1)S(1)}, bf16[768,256]{1,0:T(8,128)(2,1)S(1)}, u32[]{:S(2)}, u32[]{:S(2)}) collective-permute-start(bf16[768,256]{1,0:T(8,128)(2,1)S(1)} %collective-permute-done.4), channel_id=1, source_target_pairs={{0,1},{1,2},{2,3},{3,4},{4,5},{5,6},{6,7},{7,0},{8,9},{9,10},{10,1... | collective-permute-start | bytes 1179656 | tf_op jit(solution)/shard_map/ppermute | solution.py:34
  94.7 9.0 %collective-permute-start.6 = (bf16[768,256]{1,0:T(8,128)(2,1)S(1)}, bf16[768,256]{1,0:T(8,128)(2,1)S(1)}, u32[]{:S(2)}, u32[]{:S(2)}) collective-permute-start(bf16[768,256]{1,0:T(8,128)(2,1)S(1)} %collective-permute-done.5), channel_id=1, source_target_pairs={{0,1},{1,2},{2,3},{3,4},{4,5},{5,6},{6,7},{7,0},{8,9},{9,10},{10,1... | collective-permute-start | bytes 1179656 | tf_op jit(solution)/shard_map/ppermute | solution.py:34
  104.1 2.2 %copy-start.2 = (bf16[1,2048,1024]{2,1,0:T(8,128)(2,1)S(1)}, bf16[1,2048,1024]{2,1,0:T(8,128)(2,1)}, u32[]{:S(2)}) copy-start(bf16[1,2048,1024]{2,1,0:T(8,128)(2,1)} %param.10) | copy-start | bytes 12582916
  106.3 3.4 %copy-start.3 = (bf16[1,2048,1024]{2,1,0:T(8,128)(2,1)S(1)}, bf16[1,2048,1024]{2,1,0:T(8,128)(2,1)}, u32[]{:S(2)}) copy-start(bf16[1,2048,1024]{2,1,0:T(8,128)(2,1)} %param.11) | copy-start | bytes 12582916
  109.7 3.6 %copy-start.4 = (bf16[1,1024,2048]{2,1,0:T(8,128)(2,1)S(1)}, bf16[1,1024,2048]{2,1,0:T(8,128)(2,1)}, u32[]{:S(2)}) copy-start(bf16[1,1024,2048]{2,1,0:T(8,128)(2,1)} %param.12) | copy-start | bytes 12582916
  113.4 45.7 %copy-start = (f32[256,2]{0,1:T(2,128)S(1)}, f32[256,2]{0,1:T(2,128)}, u32[]{:S(2)}) copy-start(f32[256,2]{0,1:T(2,128)} %param.14) | copy-start | bytes 6148
  113.4 67.8 %copy-start.1 = (f32[256]{0:T(256)S(1)}, f32[256]{0:T(256)}, u32[]{:S(2)}) copy-start(f32[256]{0:T(256)} %param.15) | copy-start | bytes 3076
  155.4 9.5 %all-to-all-start.1 = ((bf16[256,4,192]{0,2,1:T(8,128)(2,1)}), bf16[256,4,192]{0,2,1:T(8,128)(2,1)S(1)}, u32[]{:S(2)}, u32[]{:S(2)}) async-start(bf16[256,4,192]{0,2,1:T(8,128)(2,1)} %bitcast.85), calls=%async_computation.2 | async-start | bytes 786432 | tf_op jit(solution)/shard_map/all_to_all | solution.py:54
Sparse Core Ops, SparseCore 0:
  118.4 37.0 reduce-scatter.1
